TPU v7x, 32 devices: a whole 2x2x4 slice. The times are simulated.
32 devices in a mesh: fs: 4 (over z), rep: 4 (over y, x), tp: 2 (over core).
Axes of the slice: x: 2, y: 2, z: 4, core: 2. Of those that a mesh axis runs over, the one named last changes fastest.
Arguments:
- saved_input: bfloat16 [16384, 2048], P(('fs', 'rep')), may hold values from -6 to 6
- value_cotangent: bfloat16 [16384, 4096], P(('fs', 'rep'), 'tp'), may hold values from -0.0061950684 to 0.0061950684
- factor: bfloat16 [2048, 128], P('fs'), may hold values from -1.5 to 1.5
- weight: float32 [2048, 4096], P('fs', 'tp'), may hold values from -1.2 to 1.2
- first_moment: float32 [128, 4096], P('fs', 'tp'), may hold values from -1.8 to 1.8
- second_moment: float32 [128, 4096], P('fs', 'tp'), may hold values from 0.1 to 1
Outputs:
- low_grad: float32 [128, 4096], P('fs', 'tp')
- new_first: float32 [128, 4096], P('fs', 'tp')
- new_second: float32 [128, 4096], P('fs', 'tp')
- direction: float32 [2048, 4096], P('fs', 'tp')
- new_weight: float32 [2048, 4096], P('fs', 'tp')
- new_copy: bfloat16 [2048, 4096], P('fs', 'tp')
All inputs are finite; a program needn't handle non-finite values.
Results may differ from a plain program's by a relative error of at most 0.006.
Values may be sent and summed in bfloat16 or wider, within the bound.
A program may use at most 64 MiB of HBM per device.

v0:
```python
import jax
import jax.numpy as jnp
from jax import lax
from jax.sharding import PartitionSpec as P

D = 2048
E = 4096
first_decay = 0.9
second_decay = 0.9
learn_rate = 0.05
epsilon = 1e-08


def on_device(saved_input, value_cotangent, factor, weight, first_moment, second_moment):
    factor_wide = factor.astype(jnp.float32)
    factor_whole = lax.all_gather(factor, "fs", axis=0, tiled=True)
    projected = jnp.dot(saved_input, factor_whole, preferred_element_type=jnp.float32)
    upper = projected.astype(jnp.bfloat16)
    lower = (projected - upper.astype(jnp.float32)).astype(jnp.bfloat16)
    dims = (((0,), (0,)), ((), ()))
    high_part = lax.dot_general(upper, value_cotangent, dims, preferred_element_type=jnp.float32)
    low_part = lax.dot_general(lower, value_cotangent, dims, preferred_element_type=jnp.float32)
    low_grad = lax.psum_scatter(high_part + low_part, "fs", scatter_dimension=0, tiled=True)
    low_grad = lax.psum(low_grad, "rep")
    new_first = first_decay * first_moment + (1.0 - first_decay) * low_grad
    new_second = second_decay * second_moment + (1.0 - second_decay) * low_grad * low_grad
    ratio = new_first / (jnp.sqrt(new_second) + epsilon)
    ratio_whole = lax.all_gather(ratio, "fs", axis=0, tiled=True)
    raw = jnp.dot(factor_wide, ratio_whole, precision=lax.Precision.HIGHEST)
    total = lax.psum(jnp.sum(raw * raw), ("fs", "tp"))
    spread = jnp.sqrt(total / (D * E))
    direction = raw / (spread + 1.0)
    new_weight = weight - learn_rate * direction
    return (low_grad, new_first, new_second, direction, new_weight, new_weight.astype(jnp.bfloat16))


def solution(mesh):
    placed = (
        P(("fs", "rep"), None),
        P(("fs", "rep"), "tp"),
        P("fs", None),
        P("fs", "tp"),
        P("fs", "tp"),
        P("fs", "tp"),
    )
    return jax.shard_map(
        on_device,
        mesh=mesh,
        in_specs=placed,
        out_specs=(
            P("fs", "tp"),
            P("fs", "tp"),
            P("fs", "tp"),
            P("fs", "tp"),
            P("fs", "tp"),
            P("fs", "tp"),
        ),
        check_vma=False,
    )
```

profile of v0, /device:TPU:0, one launch (start us, length us, event | category | flops | bytes accessed | tf_op | source)
XLA Modules:
  0.0 185.3 jit_solution(11213346444921834174)
XLA Ops:
  7.2 0.0 reduce-scatter.2.cloned.1.call-start
  7.2 0.0 copy-start
  7.2 17.7 %all_gather.6 = bf16[2048,128]{1,0:T(8,128)(2,1)S(1)} all-gather(bf16[512,128]{1,0:T(8,128)(2,1)} %param.8), channel_id=1, replica_groups=mesh['fs'=4,'rep'=4,'tp'=2] {'fs'}, dimensions={0}, use_global_device_ids=true | all-gather | bytes 655360 | tf_op jit(solution)/shard_map/all_gather | solution.py:16
  24.9 3.4 %fusion.6 = f32[1024,128]{1,0:T(8,128)S(1)} fusion(bf16[1024,2048]{1,0:T(8,128)(2,1)} %param.6, bf16[2048,128]{1,0:T(8,128)(2,1)S(1)} %all_gather.6), kind=kOutput, calls=%fused_computation.13 | convolution fusion | flops 536870912 | bytes 5242880 | tf_op jit(solution)/shard_map/dot_general | solution.py:17
  28.4 0.0 copy-done
  28.4 0.7 fusion.2
  29.1 0.0 copy-start.3
  29.1 0.0 copy-start.4
  29.2 1.7 convolution_add_fusion
  30.9 0.0 reduce-scatter.2.cloned.1.call-update
  30.9 0.0 all-reduce.2.cloned.1.call-start
  31.0 29.2 %reduce-scatter.2.cloned.1.call-done = f32[32,2048]{1,0:T(8,128)} async-done(((f32[128,2048]{1,0:T(8,128)}), f32[32,2048]{1,0:T(8,128)}) %reduce-scatter.2.cloned.1.call-update) | async-done | bytes 262160 | tf_op jit(solution)/shard_map/reduce_scatter | solution.py:23
  60.1 0.0 all-reduce.2.cloned.1.call-update
  60.1 0.0 all-gather.2.cloned.1.call-start
  60.2 44.5 %all-reduce.2.cloned.1.call-done = f32[32,2048]{1,0:T(8,128)} async-done(((f32[32,2048]{1,0:T(8,128)}), f32[32,2048]{1,0:T(8,128)}) %all-reduce.2.cloned.1.call-update) | async-done | bytes 262160 | tf_op jit(solution)/shard_map/psum | solution.py:24
  104.6 0.0 copy-done.3
  104.6 0.0 copy-done.4
  104.6 1.9 %add_divide_fusion = (f32[32,2048]{1,0:T(8,128)}, f32[32,2048]{1,0:T(8,128)}, f32[32,2048]{1,0:T(8,128)}) fusion(f32[32,2048]{1,0:T(8,128)} %all-reduce.2.cloned.1.call-done, f32[32,2048]{1,0:T(8,128)S(1)} %copy-done.3, f32[32,2048]{1,0:T(8,128)S(1)} %copy-done.4), kind=kLoop, calls=%fused_computation.8 | loop fusion | flops 524288 | bytes 1572864 | tf_op jit(solution)/shard_map/div | solution.py:27
  106.5 0.0 all-gather.2.cloned.1.call-update
  106.6 0.0 copy-start.2
  106.6 5.4 %copy.12 = f32[512,2048]{0,1:T(8,128)} copy(f32[512,2048]{1,0:T(8,128)} %param.9) | data formatting | bytes 8388608 | tf_op args[3]
  112.0 22.8 %all-gather.2.cloned.1.call-done = f32[128,2048]{1,0:T(8,128)} async-done(((f32[32,2048]{1,0:T(8,128)}), f32[128,2048]{1,0:T(8,128)}) %all-gather.2.cloned.1.call-update) | async-done | bytes 1048592 | tf_op jit(solution)/shard_map/all_gather | solution.py:28
  134.8 0.0 copy-done.2
  134.8 6.0 %multiply_reduce_fusion = (f32[]{:T(128)}, f32[2048,512]{1,0:T(8,128)}) fusion(f32[128,2048]{1,0:T(8,128)} %all-gather.2.cloned.1.call-done, bf16[512,128]{1,0:T(8,128)(2,1)S(1)} %copy-done.2), kind=kOutput, calls=%fused_computation.2 | convolution fusion | flops 1612709888 | bytes 5373956 | tf_op jit(solution)/shard_map/dot_general | solution.py:29
  140.8 15.3 %psum.15 = f32[]{:T(128)} all-reduce(f32[]{:T(128)} %get-tuple-element.18), channel_id=1, replica_groups=mesh['fs'=4,'rep'=4,'tp'=2] {'fs','tp'}, use_global_device_ids=true, to_apply=%region_3.0 | all-reduce | flops 1 | bytes 8 | tf_op jit(solution)/shard_map/psum | solution.py:30
  156.7 8.3 %fusion.4 = (bf16[512,2048]{0,1:T(8,128)(2,1)S(1)}, f32[512,2048]{0,1:T(8,128)}, f32[512,2048]{0,1:T(8,128)}) fusion(f32[512,2048]{0,1:T(8,128)} %copy.12, f32[2048,512]{1,0:T(8,128)} %get-tuple-element.19, f32[]{:T(128)S(6)} %add.29), kind=kLoop, calls=%fused_computation.12 | loop fusion | flops 4194304 | bytes 18874372 | tf_op jit(solution)/shard_map/convert_element_type | solution.py:34
  165.0 2.4 %copy.15 = bf16[512,2048]{1,0:T(8,128)(2,1)} copy(bf16[512,2048]{0,1:T(8,128)(2,1)S(1)} %get-tuple-element.12) | data formatting | bytes 4194304
  167.4 5.3 %copy.14 = f32[512,2048]{1,0:T(8,128)} copy(f32[512,2048]{0,1:T(8,128)} %get-tuple-element.13) | data formatting | bytes 8388608
  172.7 0.0 copy-start.1
  172.7 5.4 %copy.13 = f32[512,2048]{1,0:T(8,128)} copy(f32[512,2048]{0,1:T(8,128)} %get-tuple-element.14) | data formatting | bytes 8388608
  178.1 0.0 copy-done.1
  178.1 0.7 copy.17
Async XLA Ops:
  7.2 52.9 %reduce-scatter.2.cloned.1.call-start = ((), (), s32[]{:S(2)}) async-start(), calls=%async_computation.1 | async-start | bytes 1310720 | tf_op jit(solution)/shard_map/reduce_scatter | solution.py:23
  7.2 21.2 %copy-start = (bf16[1024,2048]{1,0:T(8,128)(2,1)S(1)}, bf16[1024,2048]{1,0:T(8,128)(2,1)}, u32[]{:S(2)}) copy-start(bf16[1024,2048]{1,0:T(8,128)(2,1)} %param.7) | copy-start | bytes 12582916
  29.1 75.5 %copy-start.3 = (f32[32,2048]{1,0:T(8,128)S(1)}, f32[32,2048]{1,0:T(8,128)}, u32[]{:S(2)}) copy-start(f32[32,2048]{1,0:T(8,128)} %param.11) | copy-start | bytes 786436
  29.1 75.5 %copy-start.4 = (f32[32,2048]{1,0:T(8,128)S(1)}, f32[32,2048]{1,0:T(8,128)}, u32[]{:S(2)}) copy-start(f32[32,2048]{1,0:T(8,128)} %param.10) | copy-start | bytes 786436
  30.9 73.7 %all-reduce.2.cloned.1.call-start = ((), (), s32[]{:S(2)}) async-start(), calls=%async_computation.2 | async-start | bytes 524288 | tf_op jit(solution)/shard_map/psum | solution.py:24
  60.1 74.7 %all-gather.2.cloned.1.call-start = ((), (), s32[]{:S(2)}) async-start(), calls=%async_computation.3 | async-start | bytes 1310720 | tf_op jit(solution)/shard_map/all_gather | solution.py:28
  106.6 28.2 %copy-start.2 = (bf16[512,128]{1,0:T(8,128)(2,1)S(1)}, bf16[512,128]{1,0:T(8,128)(2,1)}, u32[]{:S(2)}) copy-start(bf16[512,128]{1,0:T(8,128)(2,1)} %param.8) | copy-start | bytes 393220
  172.7 5.4 %copy-start.1 = (f32[32,2048]{1,0:T(8,128)S(1)}, f32[32,2048]{1,0:T(8,128)}, u32[]{:S(2)}) copy-start(f32[32,2048]{1,0:T(8,128)} %all-reduce.2.cloned.1.call-done) | copy-start | bytes 786436
Sparse Core Ops, SparseCore 0:
  31.0 29.0 reduce-scatter.1
  63.0 41.5 all-reduce.1
  106.8 27.9 all-gather.1
where the time goes:
time: 186 us; the launch traced here: 185 us
  waiting for transfers between devices  96.5 us (52%)
  blocking collectives  33 us (18%)
  local copies, waits for them, and re-layouts  19.2 us (10%)
  between operations  14.5 us (8%)
  matrix products  11.9 us (6%)
  other arithmetic  10.2 us (5%)
    psum x1, waiting for transfers between devices, on_device(): low_grad = lax.psum(low_grad, 'rep')  44.5 us
    reduce_scatter x1, waiting for transfers between devices, on_device(): lax.psum_scatter(high_part + low_part, 'fs', scatter_dimension=0, tiled=T...  29.2 us
    all_gather x1, waiting for transfers between devices, on_device(): ratio_whole = lax.all_gather(ratio, 'fs', axis=0, tiled=True)  22.8 us
    unnamed x15, local copies, waits for them, and re-layouts  19.2 us
    all_gather x1, blocking collectives, on_device(): factor_whole = lax.all_gather(factor, 'fs', axis=0, tiled=True)  17.7 us
    psum x1, blocking collectives, on_device(): total = lax.psum(jnp.sum(raw * raw), ('fs', 'tp'))  15.3 us
    convert_element_type x1, other arithmetic, on_device(): new_weight.astype(jnp.bfloat16)  8.28 us
    dot_general x1, matrix products, on_device(): raw = jnp.dot(factor_wide, ratio_whole, precision=lax.Precision.HIGHEST)  5.95 us
  transfers between devices with their start and end apart: 3, of which 3 were waited for; matrix products, arithmetic and copies ran while one was open for 3% of the time, Pallas kernels for 0%

commit v1 on v0

--- a/solution.py
+++ b/solution.py
@@ -2,6 +2,7 @@
 import jax.numpy as jnp
 from jax import lax
 from jax.sharding import PartitionSpec as P
+from jax.lax import axis_size, ppermute
 
 D = 2048
 E = 4096
@@ -21,7 +22,22 @@
     high_part = lax.dot_general(upper, value_cotangent, dims, preferred_element_type=jnp.float32)
     low_part = lax.dot_general(lower, value_cotangent, dims, preferred_element_type=jnp.float32)
     low_grad = lax.psum_scatter(high_part + low_part, "fs", scatter_dimension=0, tiled=True)
-    low_grad = lax.psum(low_grad, "rep")
+
+    def _produce_samples_all(a0, peer_axis):
+        lanes = axis_size(peer_axis)
+
+        def keep_up_sources_all_by_axis(new, vec_out):
+            if vec_out >= lanes:
+                return new
+            then = range(lanes)
+            b_now = map(lambda ii: (ii, ii ^ vec_out), then)
+            odd = list(b_now)
+            row_out = ppermute(new, peer_axis, odd)
+            return keep_up_sources_all_by_axis(new + row_out, 2 * vec_out)
+
+        return keep_up_sources_all_by_axis(a0, 1)
+
+    low_grad = _produce_samples_all(low_grad, "rep")
     new_first = first_decay * first_moment + (1.0 - first_decay) * low_grad
     new_second = second_decay * second_moment + (1.0 - second_decay) * low_grad * low_grad
     ratio = new_first / (jnp.sqrt(new_second) + epsilon)

time: 186 us -> 155 us (0.83)
  waiting for transfers between devices: 96.5 us -> 62.8 us
  starting transfers between devices: 0.12 us -> 3.09 us
    psum x1 -> x0, waiting for transfers between devices: 44.5 us -> none  [on_device(): low_grad = lax.psum(low_grad, 'rep')]
    ppermute x0 -> x2, waiting for transfers between devices: none -> 11.7 us  [keep_up_sources_all_by_axis(): row_out = ppermute(new, peer_axis, odd)]
    ppermute x0 -> x2, starting transfers between devices: none -> 3.01 us  [keep_up_sources_all_by_axis(): row_out = ppermute(new, peer_axis, odd)]
    unnamed x15 -> x12, local copies, waits for them, and re-layouts: 19.2 us -> 18.4 us
  transfers between devices with their start and end apart: 3 -> 4, of which waited for: 3 -> 4; matrix products, arithmetic and copies ran while one was open for 3% -> 3% of each run, Pallas kernels for 0% -> 0%
where the time goes in v1:
time: 155 us; the launch traced here: 154 us
  waiting for transfers between devices  62.8 us (41%)
  blocking collectives  33 us (21%)
  local copies, waits for them, and re-layouts  18.4 us (12%)
  between operations  14.8 us (10%)
  matrix products  11.8 us (8%)
  other arithmetic  10.3 us (7%)
  starting transfers between devices  3.09 us (2%)
    reduce_scatter x1, waiting for transfers between devices, on_device(): lax.psum_scatter(high_part + low_part, 'fs', scatter_dimension=0, tiled=T...  29.2 us
    all_gather x1, waiting for transfers between devices, on_device(): ratio_whole = lax.all_gather(ratio, 'fs', axis=0, tiled=True)  21.9 us
    unnamed x12, local copies, waits for them, and re-layouts  18.4 us
    all_gather x1, blocking collectives, on_device(): factor_whole = lax.all_gather(factor, 'fs', axis=0, tiled=True)  17.7 us
    psum x1, blocking collectives, on_device(): total = lax.psum(jnp.sum(raw * raw), ('fs', 'tp'))  15.3 us
    ppermute x2, waiting for transfers between devices, keep_up_sources_all_by_axis(): row_out = ppermute(new, peer_axis, odd)  11.7 us
    convert_element_type x1, other arithmetic, on_device(): new_weight.astype(jnp.bfloat16)  8.28 us
    dot_general x1, matrix products, on_device(): raw = jnp.dot(factor_wide, ratio_whole, precision=lax.Precision.HIGHEST)  5.95 us
  transfers between devices with their start and end apart: 4, of which 4 were waited for; matrix products, arithmetic and copies ran while one was open for 3% of the time, Pallas kernels for 0%

profile of v1, /device:TPU:0, one launch (start us, length us, event | category | flops | bytes accessed | tf_op | source)
XLA Modules:
  0.0 154.3 jit_solution(117610168198061486)
XLA Ops:
  7.2 0.0 reduce-scatter.2.cloned.1.call-start
  7.2 0.0 copy-start
  7.2 17.7 %all_gather.6 = bf16[2048,128]{1,0:T(8,128)(2,1)S(1)} all-gather(bf16[512,128]{1,0:T(8,128)(2,1)} %param.8), channel_id=1, replica_groups=mesh['fs'=4,'rep'=4,'tp'=2] {'fs'}, dimensions={0}, use_global_device_ids=true | all-gather | bytes 655360 | tf_op jit(solution)/shard_map/all_gather | solution.py:17
  24.9 3.4 %fusion.6 = f32[1024,128]{1,0:T(8,128)S(1)} fusion(bf16[1024,2048]{1,0:T(8,128)(2,1)} %param.6, bf16[2048,128]{1,0:T(8,128)(2,1)S(1)} %all_gather.6), kind=kOutput, calls=%fused_computation.13 | convolution fusion | flops 536870912 | bytes 5242880 | tf_op jit(solution)/shard_map/dot_general | solution.py:18
  28.4 0.0 copy-done
  28.4 0.7 fusion.2
  29.1 0.0 copy-start.2
  29.1 0.0 copy-start.3
  29.2 1.7 %convolution_add_fusion = f32[128,2048]{1,0:T(8,128)} fusion(f32[128,2048]{1,0:T(8,128)S(1)} %fusion.2, bf16[1024,2048]{1,0:T(8,128)(2,1)S(1)} %copy-done, f32[1024,128]{1,0:T(8,128)S(1)} %fusion.6), kind=kOutput, calls=%fused_computation.3 | convolution fusion | flops 537657344 | bytes 6815744 | tf_op jit(solution)/shard_map/dot_general | solution.py:23
  30.9 0.0 reduce-scatter.2.cloned.1.call-update
  30.9 0.0 all-gather.2.cloned.1.call-start
  31.0 29.2 %reduce-scatter.2.cloned.1.call-done = f32[32,2048]{1,0:T(8,128)} async-done(((f32[128,2048]{1,0:T(8,128)}), f32[32,2048]{1,0:T(8,128)}) %reduce-scatter.2.cloned.1.call-update) | async-done | bytes 262160 | tf_op jit(solution)/shard_map/reduce_scatter | solution.py:24
  60.1 1.5 collective-permute-start
  61.6 6.4 %collective-permute-done = f32[32,2048]{1,0:T(8,128)S(1)} collective-permute-done((f32[32,2048]{1,0:T(8,128)}, f32[32,2048]{1,0:T(8,128)S(1)}, u32[]{:S(2)}, u32[]{:S(2)}) %collective-permute-start) | collective-permute-done | bytes 262176 | tf_op jit(solution)/shard_map/ppermute | solution.py:35
  68.0 1.0 add.29
  69.0 1.5 %collective-permute-start.1 = (f32[32,2048]{1,0:T(8,128)S(1)}, f32[32,2048]{1,0:T(8,128)S(1)}, u32[]{:S(2)}, u32[]{:S(2)}) collective-permute-start(f32[32,2048]{1,0:T(8,128)S(1)} %add.29), channel_id=1, source_target_pairs={{0,4},{2,6},{4,0},{6,2},{1,5},{3,7},{5,1},{7,3},{8,12},{10,14},{12... | collective-permute-start | bytes 786440 | tf_op jit(solution)/shard_map/ppermute | solution.py:35
  70.5 5.3 %collective-permute-done.1 = f32[32,2048]{1,0:T(8,128)S(1)} collective-permute-done((f32[32,2048]{1,0:T(8,128)S(1)}, f32[32,2048]{1,0:T(8,128)S(1)}, u32[]{:S(2)}, u32[]{:S(2)}) %collective-permute-start.1) | collective-permute-done | bytes 262176 | tf_op jit(solution)/shard_map/ppermute | solution.py:35
  75.8 0.0 copy-done.2
  75.8 0.0 copy-done.3
  75.8 1.0 add_divide_fusion
  76.8 0.0 all-gather.2.cloned.1.call-update
  76.9 0.0 copy-start.1
  76.9 5.4 %copy.12 = f32[512,2048]{0,1:T(8,128)} copy(f32[512,2048]{1,0:T(8,128)} %param.9) | data formatting | bytes 8388608 | tf_op args[3]
  82.3 21.9 %all-gather.2.cloned.1.call-done = f32[128,2048]{1,0:T(8,128)} async-done(((f32[32,2048]{1,0:T(8,128)}), f32[128,2048]{1,0:T(8,128)}) %all-gather.2.cloned.1.call-update) | async-done | bytes 1048592 | tf_op jit(solution)/shard_map/all_gather | solution.py:44
  104.2 0.0 copy-done.1
  104.2 6.0 %multiply_reduce_fusion = (f32[]{:T(128)}, f32[2048,512]{1,0:T(8,128)}) fusion(f32[128,2048]{1,0:T(8,128)} %all-gather.2.cloned.1.call-done, bf16[512,128]{1,0:T(8,128)(2,1)S(1)} %copy-done.1), kind=kOutput, calls=%fused_computation.2 | convolution fusion | flops 1612709888 | bytes 5373956 | tf_op jit(solution)/shard_map/dot_general | solution.py:45
  110.1 15.3 %psum.7 = f32[]{:T(128)} all-reduce(f32[]{:T(128)} %get-tuple-element.19), channel_id=1, replica_groups=mesh['fs'=4,'rep'=4,'tp'=2] {'fs','tp'}, use_global_device_ids=true, to_apply=%region_2.0 | all-reduce | flops 1 | bytes 8 | tf_op jit(solution)/shard_map/psum | solution.py:46
  126.1 8.3 %fusion.4 = (bf16[512,2048]{0,1:T(8,128)(2,1)S(1)}, f32[512,2048]{0,1:T(8,128)}, f32[512,2048]{0,1:T(8,128)}) fusion(f32[512,2048]{0,1:T(8,128)} %copy.12, f32[2048,512]{1,0:T(8,128)} %get-tuple-element.20, f32[]{:T(128)S(6)} %add.35), kind=kLoop, calls=%fused_computation.12 | loop fusion | flops 4194304 | bytes 18874372 | tf_op jit(solution)/shard_map/convert_element_type | solution.py:50
  134.4 2.4 %copy.15 = bf16[512,2048]{1,0:T(8,128)(2,1)} copy(bf16[512,2048]{0,1:T(8,128)(2,1)S(1)} %get-tuple-element.12) | data formatting | bytes 4194304
  136.8 5.3 %copy.14 = f32[512,2048]{1,0:T(8,128)} copy(f32[512,2048]{0,1:T(8,128)} %get-tuple-element.13) | data formatting | bytes 8388608
  142.1 5.3 %copy.13 = f32[512,2048]{1,0:T(8,128)} copy(f32[512,2048]{0,1:T(8,128)} %get-tuple-element.14) | data formatting | bytes 8388608
Async XLA Ops:
  7.2 52.9 %reduce-scatter.2.cloned.1.call-start = ((), (), s32[]{:S(2)}) async-start(), calls=%async_computation.1 | async-start | bytes 1310720 | tf_op jit(solution)/shard_map/reduce_scatter | solution.py:24
  7.2 21.2 %copy-start = (bf16[1024,2048]{1,0:T(8,128)(2,1)S(1)}, bf16[1024,2048]{1,0:T(8,128)(2,1)}, u32[]{:S(2)}) copy-start(bf16[1024,2048]{1,0:T(8,128)(2,1)} %param.7) | copy-start | bytes 12582916
  29.1 46.7 %copy-start.2 = (f32[32,2048]{1,0:T(8,128)S(1)}, f32[32,2048]{1,0:T(8,128)}, u32[]{:S(2)}) copy-start(f32[32,2048]{1,0:T(8,128)} %param.11) | copy-start | bytes 786436
  29.1 46.7 %copy-start.3 = (f32[32,2048]{1,0:T(8,128)S(1)}, f32[32,2048]{1,0:T(8,128)}, u32[]{:S(2)}) copy-start(f32[32,2048]{1,0:T(8,128)} %param.10) | copy-start | bytes 786436
  30.9 73.3 %all-gather.2.cloned.1.call-start = ((), (), s32[]{:S(2)}) async-start(), calls=%async_computation.2 | async-start | bytes 1310720 | tf_op jit(solution)/shard_map/all_gather | solution.py:44
  60.1 7.9 %collective-permute-start = (f32[32,2048]{1,0:T(8,128)}, f32[32,2048]{1,0:T(8,128)S(1)}, u32[]{:S(2)}, u32[]{:S(2)}) collective-permute-start(f32[32,2048]{1,0:T(8,128)} %reduce-scatter.2.cloned.1.call-done), channel_id=1, source_target_pairs={{0,2},{2,0},{4,6},{6,4},{1,3},{3,1},{5,7},{7,5},{8,10},{10,8},{12,... | collective-permute-start | bytes 786440 | tf_op jit(solution)/shard_map/ppermute | solution.py:35
  69.0 6.8 %collective-permute-start.1 = (f32[32,2048]{1,0:T(8,128)S(1)}, f32[32,2048]{1,0:T(8,128)S(1)}, u32[]{:S(2)}, u32[]{:S(2)}) collective-permute-start(f32[32,2048]{1,0:T(8,128)S(1)} %add.29), channel_id=1, source_target_pairs={{0,4},{2,6},{4,0},{6,2},{1,5},{3,7},{5,1},{7,3},{8,12},{10,14},{12... | collective-permute-start | bytes 786440 | tf_op jit(solution)/shard_map/ppermute | solution.py:35
  76.9 27.3 %copy-start.1 = (bf16[512,128]{1,0:T(8,128)(2,1)S(1)}, bf16[512,128]{1,0:T(8,128)(2,1)}, u32[]{:S(2)}) copy-start(bf16[512,128]{1,0:T(8,128)(2,1)} %param.8) | copy-start | bytes 393220
Sparse Core Ops, SparseCore 0:
  31.0 29.0 reduce-scatter.1
  77.0 27.1 all-gather.1
